TPU v7x, 32 devices: a whole 2x2x4 slice. The times are simulated.
32 devices in a mesh: grp: 2 (over y), sp: 4 (over z), tp: 4 (over x, core).
Axes of the slice: x: 2, y: 2, z: 4, core: 2. Of those that a mesh axis runs over, the one named last changes fastest.
Arguments:
- stream_in: bfloat16 [4096, 2048], P(('grp', 'sp')), parts along dimension 0, may hold values from -6 to 6
- query_wide: bfloat16 [4096, 1024], P(('grp', 'sp'), 'tp'), parts along dimension 0, may hold values from -6 to 6
- key_wide: bfloat16 [4096, 1024], P(('grp', 'sp'), 'tp'), parts along dimension 0, may hold values from -6 to 6
- value_wide: bfloat16 [4096, 2048], P(('grp', 'sp'), 'tp'), parts along dimension 0, may hold values from -6 to 6
- query_narrow: bfloat16 [4096, 512], P(('grp', 'sp'), 'tp'), parts along dimension 0, may hold values from -6 to 6
- key_narrow: bfloat16 [4096, 512], P(('grp', 'sp'), 'tp'), parts along dimension 0, may hold values from -6 to 6
- value_narrow: bfloat16 [4096, 1024], P(('grp', 'sp'), 'tp'), parts along dimension 0, may hold values from -6 to 6
- decay_wide: float32 [4, 4096], P('tp', ('grp', 'sp')), parts along dimension 1, may hold values from -1 to 0
- decay_narrow: float32 [4, 4096], P('tp', ('grp', 'sp')), parts along dimension 1, may hold values from -1 to 0
- gain_wide: float32 [2048], P('tp'), may hold values from 0.1 to 1.9
- gain_narrow: float32 [1024], P('tp'), may hold values from 0.1 to 1.9
- out_wide: bfloat16 [2048, 2048], P('tp'), may hold values from -0.109375 to 0.109375
- out_narrow: bfloat16 [1024, 2048], P('tp'), may hold values from -0.109375 to 0.109375
- mlp_gain: float32 [2048], replicated, may hold values from 0.1 to 1.9
- up_weight: bfloat16 [2048, 8192], P('sp', 'tp'), may hold values from -0.125 to 0.125
- down_weight: bfloat16 [8192, 2048], P('tp', 'sp'), may hold values from -0.0625 to 0.0625
Outputs:
- stream_out: bfloat16 [4096, 2048], P(('grp', 'sp', 'tp')), parts along dimension 0
There are 2 independent parts, one for each index of `grp`. A program takes and returns all parts, laid end to end along the dimension named above; an argument that names none is the same for every part. Nothing has to cross between parts.
All inputs are finite; a program needn't handle non-finite values.
Results may differ from a plain program's by a relative error of at most 0.019.
Values may be sent and summed in bfloat16 or wider, within the bound.
A program may use at most 128 MiB of HBM per device.

v0:
```python
import jax
import jax.numpy as jnp
from jax import lax
from jax.sharding import PartitionSpec as P

EPS = 1e-06


def prefix(x, axis, combine, identity):
    length, mine = (lax.axis_size(axis), lax.axis_index(axis))
    everything = jax.tree.map(
        lambda part, kind: lax.all_gather(part.astype(kind), axis),
        x,
        (jnp.bfloat16, jnp.bfloat16, jnp.bfloat16, jnp.bfloat16),
    )
    start = jax.tree.map(
        lambda part, zero: jnp.broadcast_to(jnp.asarray(zero, part.dtype), part.shape), x, identity
    )

    def step(k, before):
        reached = k < mine
        new = combine(
            before, jax.tree.map(lambda part, own: part[k].astype(own.dtype), everything, x)
        )
        return jax.tree.map(lambda a, b: jnp.where(reached, a, b), new, before)

    return lax.fori_loop(0, length, step, start)


def retain_local(queries, key_rows, value_rows, log_decay):
    total_heads = log_decay.shape[0]
    length = queries.shape[0]
    key_width = queries.shape[1] // total_heads
    value_width = value_rows.shape[1] // total_heads
    query_heads = queries.reshape(length, total_heads, key_width)
    key_heads = key_rows.reshape(length, total_heads, key_width)
    value_heads = value_rows.reshape(length, total_heads, value_width)
    cumulative = jnp.cumsum(log_decay, axis=1)
    row_index = lax.broadcasted_iota(jnp.int32, (length, length), 0)
    col_index = lax.broadcasted_iota(jnp.int32, (length, length), 1)
    causal = (row_index >= col_index)[None]
    log_gap = cumulative[:, :, None] - cumulative[:, None, :]
    fading = jnp.where(causal, jnp.exp(jnp.where(causal, log_gap, 0.0)), 0.0)
    scores = jnp.einsum("ihd,jhd->hij", query_heads, key_heads, preferred_element_type=jnp.float32)
    weights_low = (scores * key_width ** (-0.5) * fading).astype(jnp.bfloat16)
    within = jnp.einsum(
        "hij,jhe->ihe", weights_low, value_heads, preferred_element_type=jnp.float32
    )
    to_end = jnp.exp(cumulative[:, -1:] - cumulative)
    keyed = (key_heads.astype(jnp.float32) * key_width ** (-0.5) * to_end.T[:, :, None]).astype(
        jnp.bfloat16
    )
    local_state = jnp.einsum("jhd,jhe->hde", keyed, value_heads, preferred_element_type=jnp.float32)
    overall = jnp.exp(cumulative[:, -1])
    return (query_heads, cumulative, within, overall, local_state)


def finish(query_heads, cumulative, within, incoming, gain_values):
    carried = (
        jnp.einsum(
            "ihd,hde->ihe",
            query_heads.astype(jnp.float32),
            incoming,
            precision=lax.Precision.HIGHEST,
        )
        * jnp.exp(cumulative).T[:, :, None]
    )
    retained = within + carried
    centered = retained - jnp.mean(retained, axis=-1, keepdims=True)
    scaled = centered * lax.rsqrt(jnp.mean(centered * centered, axis=-1, keepdims=True) + EPS)
    return (scaled.reshape(retained.shape[0], -1) * gain_values).astype(jnp.bfloat16)


def normalize(rows, gain_values):
    values = rows.astype(jnp.float32)
    scaled = values * lax.rsqrt(jnp.mean(values * values, axis=-1, keepdims=True) + EPS)
    return (scaled * gain_values).astype(jnp.bfloat16)


def join_states(earlier, latter):
    return (
        earlier[0] * latter[0],
        latter[0][:, None, None] * earlier[1] + latter[1],
        earlier[2] * latter[2],
        latter[2][:, None, None] * earlier[3] + latter[3],
    )


def on_device(
    stream_in,
    query_wide,
    key_wide,
    value_wide,
    query_narrow,
    key_narrow,
    value_narrow,
    decay_wide,
    decay_narrow,
    gain_wide,
    gain_narrow,
    out_wide,
    out_narrow,
    mlp_gain,
    up_weight,
    down_weight,
):
    length = stream_in.shape[0]
    portion = length // lax.axis_size("tp")
    member = lax.axis_index("tp")
    wide_query, wide_cum, wide_within, wide_factor, wide_state = retain_local(
        query_wide, key_wide, value_wide, decay_wide
    )
    thin_query, thin_cum, thin_within, thin_factor, thin_state = retain_local(
        query_narrow, key_narrow, value_narrow, decay_narrow
    )
    identity = (
        jnp.ones_like(wide_factor),
        jnp.zeros_like(wide_state),
        jnp.ones_like(thin_factor),
        jnp.zeros_like(thin_state),
    )
    incoming = prefix(
        (wide_factor, wide_state, thin_factor, thin_state), "sp", join_states, identity
    )
    normed_wide = finish(wide_query, wide_cum, wide_within, incoming[1], gain_wide)
    normed_thin = finish(thin_query, thin_cum, thin_within, incoming[3], gain_narrow)
    up_full, down_full = (
        lax.all_gather(up_weight, "sp", axis=0, tiled=True),
        lax.all_gather(down_weight, "sp", axis=1, tiled=True),
    )
    mixed_heads = lax.psum(
        (
            jnp.dot(normed_wide, out_wide, preferred_element_type=jnp.float32)
            + jnp.dot(normed_thin, out_narrow, preferred_element_type=jnp.float32)
        ).astype(jnp.bfloat16),
        "tp",
    ).astype(jnp.float32)
    whole_rows = (stream_in.astype(jnp.float32) + mixed_heads).astype(jnp.bfloat16)
    raised = jax.nn.relu(
        jnp.dot(normalize(whole_rows, mlp_gain), up_full, preferred_element_type=jnp.float32)
    )
    hidden = (raised * raised).astype(jnp.bfloat16)
    middle = lax.dynamic_slice_in_dim(whole_rows, member * portion, portion, 0)
    channel = lax.psum_scatter(
        jnp.dot(hidden, down_full, preferred_element_type=jnp.float32).astype(jnp.bfloat16),
        "tp",
        scatter_dimension=0,
        tiled=True,
    ).astype(jnp.float32)
    return (middle.astype(jnp.float32) + channel).astype(jnp.bfloat16)


def solution(mesh):
    placed = (
        P(("grp", "sp"), None),
        P(("grp", "sp"), "tp"),
        P(("grp", "sp"), "tp"),
        P(("grp", "sp"), "tp"),
        P(("grp", "sp"), "tp"),
        P(("grp", "sp"), "tp"),
        P(("grp", "sp"), "tp"),
        P("tp", ("grp", "sp")),
        P("tp", ("grp", "sp")),
        P("tp"),
        P("tp"),
        P("tp", None),
        P("tp", None),
        P(),
        P("sp", "tp"),
        P("tp", "sp"),
    )
    return jax.shard_map(
        on_device,
        mesh=mesh,
        in_specs=placed,
        out_specs=P(("grp", "sp", "tp"), None),
        check_vma=False,
    )
```

profile of v0, /device:TPU:0, one launch (start us, length us, event | category | flops | bytes accessed | tf_op | source)
XLA Modules:
  0.0 481.8 jit_solution(3034267746610162179)
XLA Ops:
  6.5 1.1 reduce-window.14
  8.0 0.7 fusion.53
  11.2 2.3 convolution_convert_fusion.1
  13.6 1.0 reduce-window.16
  15.6 0.6 slice.28
  17.5 1.2 dynamic-slice
  18.7 0.7 dynamic-update-slice
  19.4 0.7 dynamic-update-slice.1
  20.1 14.0 %all-reduce.2 = (bf16[4]{0:T(256)(128)(2,1)S(1)}, bf16[4]{0:T(256)(128)(2,1)S(1)}) all-reduce(bf16[4]{0:T(256)(128)(2,1)S(1)} %dynamic-update-slice, bf16[4]{0:T(256)(128)(2,1)S(1)} %dynamic-update-slice.1), channel_id=1, replica_groups=mesh['grp'=2,'sp'=4,'tp'=4] {'sp'}, use_global_device_ids=true, to_apply=%add | all-reduce | flops 8 | bytes 32
  34.1 1.4 convolution_convert_fusion.2
  35.5 15.4 %all-gather.1 = bf16[512,256]{1,0:T(8,128)(2,1)S(1)} all-gather(bf16[128,256]{1,0:T(8,128)(2,1)S(1)} %convolution_convert_fusion.2), channel_id=3, replica_groups=mesh['grp'=2,'sp'=4,'tp'=4] {'sp'}, dimensions={0}, use_global_device_ids=true | all-gather | bytes 327680 | tf_op jit(solution)/shard_map/all_gather | solution.py:12
  50.9 1.6 fusion.15
  52.6 3.0 convolution_bitcast_fusion.1
  55.6 13.0 %while.16 = (s32[]{:T(128)}, f32[1,256,512]{2,1,0:T(8,128)S(1)}, f32[1,128,256]{2,1,0:T(8,128)S(1)}, s32[]{:T(128)}, bf16[4,1]{0,1:T(2,128)(2,1)S(1)}, /*index=5...) while((s32[]{:T(128)}, f32[1,256,512]{2,1,0:T(8,128)S(1)}, ...), condition=%wide.region_5.6_spmd.clone, body=%wide.region_4.5_spmd.clone.sunk | while | flops 819206 | bytes 1638563 | solution.py:27
  56.8 1.3 fusion.81
  58.8 0.6 constant_dynamic-slice_fusion.3
  60.1 1.3 fusion.81
  62.1 0.6 constant_dynamic-slice_fusion.3
  63.3 1.3 fusion.81
  66.6 1.3 fusion.81
  68.6 2.5 fusion.55
  71.3 1.4 fusion.54
  72.8 0.8 fusion.41
  73.6 2.8 add_convert_fusion.1
  76.6 0.7 all-gather.6.cloned.1.call-update
  78.1 48.4 %all-reduce.5.cloned.1.call-done = bf16[512,2048]{1,0:T(8,128)(2,1)} async-done(((bf16[512,2048]{1,0:T(8,128)(2,1)}), bf16[512,2048]{1,0:T(8,128)(2,1)}) %all-reduce.5.cloned.1.call-update) | async-done | bytes 2097168 | tf_op jit(solution)/shard_map/psum | solution.py:131
  126.5 4.5 fusion.2
  131.1 146.7 %all-gather.6.cloned.1.call-done = bf16[2048,2048]{1,0:T(8,128)(2,1)} async-done(((bf16[512,2048]{1,0:T(8,128)(2,1)}), bf16[2048,2048]{1,0:T(8,128)(2,1)}) %all-gather.6.cloned.1.call-update) | async-done | bytes 8388624 | tf_op jit(solution)/shard_map/all_gather | solution.py:128
  277.8 149.3 %all-gather.8.cloned.1.call-done = bf16[2048,2048]{1,0:T(8,128)(2,1)} async-done(((bf16[2048,512]{1,0:T(8,128)(2,1)}), bf16[2048,2048]{1,0:T(8,128)(2,1)}) %all-gather.8.cloned.1.call-update) | async-done | bytes 8388624 | tf_op jit(solution)/shard_map/all_gather | solution.py:129
  427.1 16.5 %convolution_convert_fusion = bf16[512,2048]{1,0:T(8,128)(2,1)} fusion(bf16[2048,2048]{1,0:T(8,128)(2,1)} %all-gather.8.cloned.1.call-done, bf16[2048,2048]{1,0:T(8,128)(2,1)} %all-gather.6.cloned.1.call-done, bf16[512,2048]{1,0:T(8,128)(2,1)} %get-tuple-element.209, f32[2048]{0:T(1024)S(1)} %copy-done.6, f32[512]{0:T(512)S(1)} %add_rsqrt_fusion), kind=kOutput, calls=%fused_computation.14 | convolution fusion | flops 8598323200 | bytes 20981760 | tf_op jit(solution)/shard_map/dot_general | solution.py:145
  443.6 29.5 %reduce-scatter.2.cloned.1.call-done = bf16[128,2048]{1,0:T(8,128)(2,1)} async-done(((bf16[512,2048]{1,0:T(8,128)(2,1)}), bf16[128,2048]{1,0:T(8,128)(2,1)}) %reduce-scatter.2.cloned.1.call-update) | async-done | bytes 524304 | tf_op jit(solution)/shard_map/reduce_scatter | solution.py:144
  473.1 2.1 add_convert_fusion.2
  (55 shorter events, 5.5 us)
Async XLA Ops:
  6.5 67.1 %copy-start = (bf16[512,2048]{1,0:T(8,128)(2,1)S(1)}, bf16[512,2048]{1,0:T(8,128)(2,1)}, u32[]{:S(2)}) copy-start(bf16[512,2048]{1,0:T(8,128)(2,1)} %param.29) | copy-start | bytes 6291460
  6.5 49.1 %all-gather.10.cloned.1.call-start = ((), (), s32[]{:S(2)}) async-start(), calls=%async_computation.5 | async-start | bytes 1310720 | tf_op jit(solution)/shard_map/all_gather | solution.py:12
  8.7 2.4 copy-start.2
  13.5 113.0 %all-reduce.5.cloned.1.call-start = ((), (), s32[]{:S(2)}) async-start(), calls=%async_computation.1 | async-start | bytes 4194304 | tf_op jit(solution)/shard_map/psum | solution.py:131
  55.6 13.0 %copy-start.3 = (f32[512]{0:T(512)S(1)}, f32[512]{0:T(512)}, u32[]{:S(2)}) copy-start(f32[512]{0:T(512)} %get-tuple-element.210) | copy-start | bytes 6148
  68.6 4.2 copy-start.1
  68.6 4.2 copy-start.4
  72.8 0.9 copy-start.5
  76.5 201.3 %all-gather.6.cloned.1.call-start = ((), (), s32[]{:S(2)}) async-start(), calls=%async_computation.2 | async-start | bytes 10485760 | tf_op jit(solution)/shard_map/all_gather | solution.py:128
  77.3 349.8 %copy-start.6 = (f32[2048]{0:T(1024)S(1)}, f32[2048]{0:T(1024)}, u32[]{:S(2)}) copy-start(f32[2048]{0:T(1024)} %param.31) | copy-start | bytes 24580
  77.3 349.8 %all-gather.8.cloned.1.call-start = ((), (), s32[]{:S(2)}) async-start(), calls=%async_computation.3 | async-start | bytes 10485760 | tf_op jit(solution)/shard_map/all_gather | solution.py:129
  77.8 395.3 %reduce-scatter.2.cloned.1.call-start = ((), (), s32[]{:S(2)}) async-start(), calls=%async_computation.4 | async-start | bytes 2621440 | tf_op jit(solution)/shard_map/reduce_scatter | solution.py:144
Sparse Core Ops, SparseCore 0:
  13.6 34.9 all-gather.9
  76.6 49.8 all-reduce.4
  128.1 149.6 all-gather.5
  279.2 147.7 all-gather.7
  443.7 29.3 reduce-scatter.1
where the time goes:
time: 482 us
  waiting for transfers between devices  375 us (78%)
  matrix products  32.3 us (7%)
  blocking collectives  29.4 us (6%)
  between operations  15.8 us (3%)
  other arithmetic  15.5 us (3%)
  local copies, waits for them, and re-layouts  8.03 us (2%)
  loops' own time  5.17 us (1%)
    all_gather x1, waiting for transfers between devices, on_device(): lax.all_gather(down_weight, 'sp', axis=1, tiled=True)  149 us
    all_gather x1, waiting for transfers between devices, on_device(): lax.all_gather(up_weight, 'sp', axis=0, tiled=True)  147 us
    psum x1, waiting for transfers between devices, on_device(): lax.psum((jnp.dot(normed_wide, out_wide, preferred_element_type=jnp.float...  48.4 us
    reduce_scatter x1, waiting for transfers between devices, on_device(): lax.psum_scatter(jnp.dot(hidden, down_full, preferred_element_type=jnp.fl...  29.5 us
    dot_general x1, matrix products, on_device(): jnp.dot(hidden, down_full, preferred_element_type=jnp.float32)  16.5 us
    all_gather x1, blocking collectives, prefix(): lax.all_gather(part.astype(kind), axis)  15.4 us
    unnamed x1, blocking collectives  14 us
  transfers between devices with their start and end apart: 5, of which 4 were waited for; matrix products, arithmetic and copies ran while one was open for 3% of the time, Pallas kernels for 0%

commit v1 on v0

--- a/solution.py
+++ b/solution.py
@@ -4,6 +4,11 @@
 from jax.sharding import PartitionSpec as P
 
 EPS = 1e-06
+
+
+def add_all(block, axis):
+    parts = lax.all_gather(block, axis)
+    return jnp.sum(parts, axis=0)
 
 
 def prefix(x, axis, combine, identity):
@@ -128,7 +133,7 @@
         lax.all_gather(up_weight, "sp", axis=0, tiled=True),
         lax.all_gather(down_weight, "sp", axis=1, tiled=True),
     )
-    mixed_heads = lax.psum(
+    mixed_heads = add_all(
         (
             jnp.dot(normed_wide, out_wide, preferred_element_type=jnp.float32)
             + jnp.dot(normed_thin, out_narrow, preferred_element_type=jnp.float32)

time: 482 us -> 489 us (1.015)
  other arithmetic: 15.5 us -> 23.4 us
    all_gather x0 -> x1, waiting for transfers between devices: none -> 55.3 us  [add_all(): parts = lax.all_gather(block, axis)]
    psum x1 -> x0, waiting for transfers between devices: 48.4 us -> none  [on_device(): lax.psum((jnp.dot(normed_wide, out_wide, preferred_element_type=jnp.float...]
    all_gather x1, waiting for transfers between devices: 149 us -> 139 us  [on_device(): lax.all_gather(down_weight, 'sp', axis=1, tiled=True)]
    reduce_sum x0 -> x1, other arithmetic: none -> 7.27 us  [add_all(): return jnp.sum(parts, axis=0)]
  transfers between devices with their start and end apart: 5 -> 5, of which waited for: 4 -> 4; matrix products, arithmetic and copies ran while one was open for 3% -> 5% of each run, Pallas kernels for 0% -> 0%
where the time goes in v1:
time: 489 us
  waiting for transfers between devices  374 us (76%)
  matrix products  32.4 us (7%)
  blocking collectives  29.4 us (6%)
  other arithmetic  23.4 us (5%)
  between operations  15.8 us (3%)
  local copies, waits for them, and re-layouts  8.03 us (2%)
  loops' own time  5.16 us (1%)
    all_gather x1, waiting for transfers between devices, on_device(): lax.all_gather(up_weight, 'sp', axis=0, tiled=True)  149 us
    all_gather x1, waiting for transfers between devices, on_device(): lax.all_gather(down_weight, 'sp', axis=1, tiled=True)  139 us
    all_gather x1, waiting for transfers between devices, add_all(): parts = lax.all_gather(block, axis)  55.3 us
    reduce_scatter x1, waiting for transfers between devices, on_device(): lax.psum_scatter(jnp.dot(hidden, down_full, preferred_element_type=jnp.fl...  29.5 us
    dot_general x1, matrix products, on_device(): jnp.dot(hidden, down_full, preferred_element_type=jnp.float32)  16.6 us
    all_gather x1, blocking collectives, prefix(): lax.all_gather(part.astype(kind), axis)  15.4 us
    unnamed x1, blocking collectives  14 us
  transfers between devices with their start and end apart: 5, of which 4 were waited for; matrix products, arithmetic and copies ran while one was open for 5% of the time, Pallas kernels for 0%

profile of v1, /device:TPU:0, one launch (start us, length us, event | category | flops | bytes accessed | tf_op | source)
XLA Modules:
  0.0 488.7 jit_solution(3423841543137919722)
XLA Ops:
  6.5 1.1 reduce-window.14
  8.0 0.7 fusion.53
  11.2 2.3 convolution_convert_fusion.1
  13.6 1.0 reduce-window.16
  15.6 0.6 slice.28
  17.5 1.2 dynamic-slice
  18.7 0.7 dynamic-update-slice
  19.4 0.7 dynamic-update-slice.1
  20.1 14.0 %all-reduce.2 = (bf16[4]{0:T(256)(128)(2,1)S(1)}, bf16[4]{0:T(256)(128)(2,1)S(1)}) all-reduce(bf16[4]{0:T(256)(128)(2,1)S(1)} %dynamic-update-slice, bf16[4]{0:T(256)(128)(2,1)S(1)} %dynamic-update-slice.1), channel_id=1, replica_groups=mesh['grp'=2,'sp'=4,'tp'=4] {'sp'}, use_global_device_ids=true, to_apply=%add | all-reduce | flops 8 | bytes 32
  34.1 1.4 convolution_convert_fusion.2
  35.5 15.4 %all-gather.1 = bf16[512,256]{1,0:T(8,128)(2,1)S(1)} all-gather(bf16[128,256]{1,0:T(8,128)(2,1)S(1)} %convolution_convert_fusion.2), channel_id=3, replica_groups=mesh['grp'=2,'sp'=4,'tp'=4] {'sp'}, dimensions={0}, use_global_device_ids=true | all-gather | bytes 327680 | tf_op jit(solution)/shard_map/all_gather | solution.py:17
  50.9 1.6 fusion.15
  52.6 3.0 convolution_bitcast_fusion.1
  55.6 13.0 %while.16 = (s32[]{:T(128)}, f32[1,256,512]{2,1,0:T(8,128)S(1)}, f32[1,128,256]{2,1,0:T(8,128)S(1)}, s32[]{:T(128)}, bf16[4,1]{0,1:T(2,128)(2,1)S(1)}, /*index=5...) while((s32[]{:T(128)}, f32[1,256,512]{2,1,0:T(8,128)S(1)}, ...), condition=%wide.region_5.6_spmd.clone, body=%wide.region_4.5_spmd.clone.sunk | while | flops 819206 | bytes 1638563 | solution.py:32
  56.8 1.3 fusion.81
  58.8 0.6 constant_dynamic-slice_fusion.3
  60.1 1.3 fusion.81
  63.3 1.3 fusion.81
  66.6 1.3 fusion.81
  68.6 2.5 fusion.55
  71.3 1.4 fusion.54
  72.8 0.8 fusion.41
  73.7 2.9 add_convert_fusion.1
  76.6 0.7 all-gather.10.cloned.1.call-update
  78.1 55.3 %all-gather.14.cloned.1.call-done = bf16[2048,2048]{1,0:T(8,128)(2,1)} async-done(((bf16[512,2048]{1,0:T(8,128)(2,1)}), bf16[2048,2048]{1,0:T(8,128)(2,1)}) %all-gather.14.cloned.1.call-update) | async-done | bytes 8388624 | tf_op jit(solution)/shard_map/all_gather | solution.py:10
  133.4 7.3 %reduce_sum.61 = bf16[512,2048]{1,0:T(8,128)(2,1)} reduce(bf16[4,512,2048]{2,1,0:T(8,128)(2,1)} %bitcast.119, bf16[]{:T(256)} %constant.63.clone.1), dimensions={0}, to_apply=%region_10.11 | reduce | flops 3145728 | bytes 10485762 | tf_op jit(solution)/shard_map/reduce_sum | solution.py:11
  140.7 5.1 %fusion.2 = (f32[512]{0:T(512)S(1)}, bf16[512,2048]{1,0:T(8,128)(2,1)}) fusion(bf16[512,2048]{1,0:T(8,128)(2,1)} %reduce_sum.61, bf16[512,2048]{1,0:T(8,128)(2,1)} %param.18), kind=kLoop, calls=%fused_computation.8 | loop fusion | flops 7339520 | bytes 6293504 | tf_op jit(solution)/shard_map/reduce_sum | solution.py:81
  145.9 138.8 %all-gather.10.cloned.1.call-done = bf16[2048,2048]{1,0:T(8,128)(2,1)} async-done(((bf16[2048,512]{1,0:T(8,128)(2,1)}), bf16[2048,2048]{1,0:T(8,128)(2,1)}) %all-gather.10.cloned.1.call-update) | async-done | bytes 8388624 | tf_op jit(solution)/shard_map/all_gather | solution.py:134
  284.7 149.3 %all-gather.8.cloned.1.call-done = bf16[2048,2048]{1,0:T(8,128)(2,1)} async-done(((bf16[512,2048]{1,0:T(8,128)(2,1)}), bf16[2048,2048]{1,0:T(8,128)(2,1)}) %all-gather.8.cloned.1.call-update) | async-done | bytes 8388624 | tf_op jit(solution)/shard_map/all_gather | solution.py:133
  433.9 16.6 %convolution_convert_fusion = bf16[512,2048]{1,0:T(8,128)(2,1)} fusion(bf16[2048,2048]{1,0:T(8,128)(2,1)} %all-gather.10.cloned.1.call-done, bf16[2048,2048]{1,0:T(8,128)(2,1)} %all-gather.8.cloned.1.call-done, bf16[512,2048]{1,0:T(8,128)(2,1)} %get-tuple-element.209, f32[2048]{0:T(1024)S(1)} %copy-done.6, f32[512]{0:T(512)S(1)} %add_rsqrt_fusion), kind=kOutput, calls=%fused_computation.14 | convolution fusion | flops 8598323200 | bytes 20981760 | tf_op jit(solution)/shard_map/dot_general | solution.py:150
  450.5 29.5 %reduce-scatter.2.cloned.1.call-done = bf16[128,2048]{1,0:T(8,128)(2,1)} async-done(((bf16[512,2048]{1,0:T(8,128)(2,1)}), bf16[128,2048]{1,0:T(8,128)(2,1)}) %reduce-scatter.2.cloned.1.call-update) | async-done | bytes 524304 | tf_op jit(solution)/shard_map/reduce_scatter | solution.py:149
  480.1 2.1 add_convert_fusion.2
  (56 shorter events, 6.1 us)
Async XLA Ops:
  6.5 67.1 %copy-start = (bf16[512,2048]{1,0:T(8,128)(2,1)S(1)}, bf16[512,2048]{1,0:T(8,128)(2,1)}, u32[]{:S(2)}) copy-start(bf16[512,2048]{1,0:T(8,128)(2,1)} %param.29) | copy-start | bytes 6291460
  6.5 49.1 %all-gather.12.cloned.1.call-start = ((), (), s32[]{:S(2)}) async-start(), calls=%async_computation.4 | async-start | bytes 1310720 | tf_op jit(solution)/shard_map/all_gather | solution.py:17
  8.7 2.4 copy-start.2
  13.5 120.0 %all-gather.14.cloned.1.call-start = ((), (), s32[]{:S(2)}) async-start(), calls=%async_computation.5 | async-start | bytes 10485760 | tf_op jit(solution)/shard_map/all_gather | solution.py:10
  55.6 13.0 %copy-start.3 = (f32[512]{0:T(512)S(1)}, f32[512]{0:T(512)}, u32[]{:S(2)}) copy-start(f32[512]{0:T(512)} %get-tuple-element.210) | copy-start | bytes 6148
  68.6 4.2 copy-start.1
  68.6 4.2 copy-start.4
  72.8 0.9 copy-start.5
  76.6 208.1 %all-gather.10.cloned.1.call-start = ((), (), s32[]{:S(2)}) async-start(), calls=%async_computation.2 | async-start | bytes 10485760 | tf_op jit(solution)/shard_map/all_gather | solution.py:134
  77.3 356.6 %all-gather.8.cloned.1.call-start = ((), (), s32[]{:S(2)}) async-start(), calls=%async_computation.1 | async-start | bytes 10485760 | tf_op jit(solution)/shard_map/all_gather | solution.py:133
  77.9 402.2 %reduce-scatter.2.cloned.1.call-start = ((), (), s32[]{:S(2)}) async-start(), calls=%async_computation.3 | async-start | bytes 2621440 | tf_op jit(solution)/shard_map/reduce_scatter | solution.py:149
  140.7 293.2 %copy-start.6 = (f32[2048]{0:T(1024)S(1)}, f32[2048]{0:T(1024)}, u32[]{:S(2)}) copy-start(f32[2048]{0:T(1024)} %param.31) | copy-start | bytes 24580
Sparse Core Ops, SparseCore 0:
  13.6 34.9 all-gather.11
  76.7 56.7 all-gather.13
  135.0 149.6 all-gather.9
  286.1 147.7 all-gather.7
  450.7 29.3 reduce-scatter.1
